TPU v7x, 128 devices: a whole 4x4x4 slice. The times are simulated.
128 devices in a mesh: fs: 32 (over z, y, core), tp: 4 (over x).
Axes of the slice: x: 4, y: 4, z: 4, core: 2. Of those that a mesh axis runs over, the one named last changes fastest.
Arguments:
- tokens: bfloat16 [49152, 2048], P('fs', 'tp'), may hold values from -6 to 6
- norm_gain: float32 [2048], P('fs'), may hold values from 0.1 to 1.9
- up_weight: float32 [2048, 8192], P('fs', 'tp'), may hold values from -0.125 to 0.125
- down_weight: float32 [2048, 8192], P('fs', 'tp'), may hold values from -0.0625 to 0.0625
Outputs:
- up_matrix: bfloat16 [2048, 8192], P(None, 'tp')
- down_matrix: bfloat16 [2048, 8192], P(None, 'tp')
- mixed: bfloat16 [49152, 2048], P('fs', 'tp')
All inputs are finite; a program needn't handle non-finite values.
Results may differ from a plain program's by a relative error of at most 0.0095.
Values may be sent and summed in bfloat16 or wider, within the bound.
A program may use at most 128 MiB of HBM per device.

v0:
```python
import jax
import jax.numpy as jnp
from jax import lax
from jax.sharding import PartitionSpec as P

epsilon = 1e-06


def sent_to_all(x, axis):
    devices = lax.axis_size(axis)
    return lax.all_to_all(jnp.broadcast_to(x[None], (devices, *x.shape)), axis, 0, 0, tiled=True)


def joined_along(pieces, dim):
    shape = list(pieces.shape[1:])
    shape[dim] *= pieces.shape[0]
    return jnp.moveaxis(pieces, 0, dim).reshape(shape)


def gather_directly(x, axis, dim):
    pieces = sent_to_all(x, axis)
    return joined_along(pieces, dim)


def side_by_side(arrays, axis, dim, along):
    both = jnp.concatenate(arrays, axis=along)
    filled, at, gathered = (lax.all_gather(both, axis, axis=dim, tiled=True), 0, [])
    for a in arrays:
        gathered.append(lax.slice_in_dim(filled, at, at + a.shape[along], axis=along))
        at += a.shape[along]
    return tuple(gathered)


def row_scale(full_rows):
    widened = full_rows.astype(jnp.float32)
    scaled = widened * lax.rsqrt(jnp.mean(widened * widened, axis=-1, keepdims=True) + epsilon)
    return scaled.astype(jnp.bfloat16)


def on_device(tokens, norm_gain, up_weight, down_weight):
    up_local = (norm_gain[:, None] * up_weight).astype(jnp.bfloat16)
    down_local = down_weight.astype(jnp.bfloat16)
    full_rows = gather_directly(tokens, "tp", 1)
    normed = row_scale(full_rows)
    up_matrix, down_matrix = side_by_side((up_local, down_local), "fs", 0, 1)
    up_values = jnp.dot(normed, up_matrix, preferred_element_type=jnp.float32)
    hidden = jnp.square(jax.nn.relu(up_values)).astype(jnp.bfloat16)
    partial_value = lax.dot_general(
        hidden, down_matrix, (((1,), (1,)), ((), ())), preferred_element_type=jnp.float32
    )
    rounded = partial_value.astype(jnp.bfloat16).astype(jnp.float32)
    mixed = lax.psum_scatter(rounded.astype(jnp.bfloat16), "tp", scatter_dimension=1, tiled=True)
    return (up_matrix, down_matrix, mixed)


def solution(mesh):
    return jax.shard_map(
        on_device,
        mesh=mesh,
        in_specs=(P("fs", "tp"), P("fs"), P("fs", "tp"), P("fs", "tp")),
        out_specs=(P(None, "tp"), P(None, "tp"), P("fs", "tp")),
        check_vma=False,
    )
```

profile of v0, /device:TPU:1, one launch (start us, length us, event | category | flops | bytes accessed | tf_op | source)
XLA Modules:
  0.0 211.9 jit_solution(18046108403022100348)
XLA Ops:
  7.2 0.0 all-gather.2.cloned.1.call-start
  7.2 1.1 convert_element_type.31
  8.3 1.1 multiply_convert_fusion.1
  9.4 0.8 pad_maximum_fusion
  10.3 0.0 all-gather.2.cloned.1.call-update
  10.3 0.0 reduce-scatter.2.cloned.1.call-start
  10.3 1.7 copy.7
  12.1 0.5 broadcast_in_dim.2
  12.5 75.0 %all_to_all.5 = bf16[4,1536,512]{1,2,0:T(8,128)(2,1)S(1)} all-to-all(bf16[4,1536,512]{1,2,0:T(8,128)(2,1)S(1)} %broadcast_in_dim.2), channel_id=1, replica_groups=mesh['fs'=32,'tp'=4] {'tp'}, dimensions={0} | all-to-all | bytes 12582912 | tf_op jit(solution)/shard_map/all_to_all | solution.py:11
  87.6 1.3 multiply_reduce_fusion
  88.9 4.0 %fusion = bf16[1536,2048]{0,1:T(8,128)(2,1)} fusion(f32[1536]{0:T(1024)S(1)} %add_rsqrt_fusion, bf16[4,1536,512]{1,2,0:T(8,128)(2,1)S(1)} %all_to_all.5), kind=kLoop, calls=%fused_computation.1 | loop fusion | flops 9437184 | bytes 12589056 | tf_op jit(solution)/shard_map/convert_element_type | solution.py:37
  92.9 0.0 all-gather.2.cloned.1.call-done
  92.9 11.9 %fusion.3 = (bf16[2048,2048]{1,0:T(8,128)(2,1)}, bf16[2048,2048]{1,0:T(8,128)(2,1)}) fusion(bf16[2048,4096]{1,0:T(8,128)(2,1)} %all-gather.2.cloned.1.call-done), kind=kLoop, calls=%fused_computation.10 | loop fusion | bytes 33554432 | tf_op jit(solution)/shard_map/slice | solution.py:29
  104.8 34.5 %convolution_convert_fusion = bf16[1536,2048]{1,0:T(8,128)(2,1)} fusion(bf16[2048,2048]{1,0:T(8,128)(2,1)} %get-tuple-element.3, bf16[1536,2048]{0,1:T(8,128)(2,1)} %fusion, bf16[2048,2048]{1,0:T(8,128)(2,1)} %get-tuple-element.4), kind=kOutput, calls=%fused_computation.4 | convolution fusion | flops 25782386688 | bytes 29360128 | tf_op jit(solution)/shard_map/dot_general | solution.py:48
  139.3 0.0 reduce-scatter.2.cloned.1.call-update
  139.3 65.7 %reduce-scatter.2.cloned.1.call-done = bf16[1536,512]{1,0:T(8,128)(2,1)} async-done(((bf16[1536,2048]{1,0:T(8,128)(2,1)}), bf16[1536,512]{1,0:T(8,128)(2,1)}) %reduce-scatter.2.cloned.1.call-update) | async-done | bytes 1572880 | tf_op jit(solution)/shard_map/reduce_scatter | solution.py:52
  (1 shorter events, 0.0 us)
Async XLA Ops:
  7.2 85.7 %all-gather.2.cloned.1.call-start = ((), (), s32[]{:S(2)}) async-start(), calls=%async_computation.2 | async-start | bytes 17301504 | tf_op jit(solution)/shard_map/all_gather | solution.py:27
  10.3 194.7 %reduce-scatter.2.cloned.1.call-start = ((), (), s32[]{:S(2)}) async-start(), calls=%async_computation.3 | async-start | bytes 7864320 | tf_op jit(solution)/shard_map/reduce_scatter | solution.py:52
Sparse Core Ops, SparseCore 0:
  10.8 76.2 all-gather.1
  139.5 65.5 reduce-scatter.1
where the time goes:
time: 212 us
  blocking collectives  75 us (35%)
  waiting for transfers between devices  65.7 us (31%)
  matrix products  34.5 us (16%)
  local copies, waits for them, and re-layouts  14.1 us (7%)
  between operations  14.1 us (7%)
  other arithmetic  8.33 us (4%)
    all_to_all x1, blocking collectives, sent_to_all(): lax.all_to_all(jnp.broadcast_to(x[None], (devices, *x.shape)), axis, 0, 0...  75 us
    reduce_scatter x1, waiting for transfers between devices, on_device(): lax.psum_scatter(rounded.astype(jnp.bfloat16), 'tp', scatter_dimension=1,...  65.7 us
    dot_general x1, matrix products, on_device(): lax.dot_general(hidden, down_matrix, (((1,), (1,)), ((), ())), preferred_...  34.5 us
    slice x1, local copies, waits for them, and re-layouts, side_by_side(): lax.slice_in_dim(filled, at, at + a.shape[along], axis=along)  11.9 us
  transfers between devices with their start and end apart: 2, of which 1 were waited for; matrix products, arithmetic and copies ran while one was open for 4% of the time, Pallas kernels for 0%

commit v1 on v0

v1 whole, which is shorter than its diff:
```python
import functools

import jax
import jax.numpy as jnp
from jax import lax
from jax.experimental import pallas as pl
from jax.experimental.pallas import tpu as pltpu
from jax.sharding import PartitionSpec as P

epsilon = 1e-06
RING = 4
HALF = 32
PIECE = 128
CHUNK = 256
MESH = pl.DeviceIdType.MESH
F32, BF16 = jnp.float32, jnp.bfloat16


def onward(at, first, second, half):
    links = []
    if at[second] == 0:
        if at[first] == 0:
            links += [(first, 1), (first, -1)]
        elif at[first] == 1 and half == 0:
            links += [(first, 1)]
        elif at[first] == -1 and half == 1:
            links += [(first, -1)]
        links += [(second, 1), (second, -1)]
    elif at[second] == 1 and half == 0:
        links += [(second, 1)]
    elif at[second] == -1 and half == 1:
        links += [(second, -1)]
    return links


def weight_plan():
    links = [(axis, sign) for axis in "yz" for sign in (1, -1)]
    queues = {link: [] for link in links}

    def offer(unit, slot):
        matrix, z, y, half = unit
        first, second = ("y", "z") if matrix == 0 else ("z", "y")
        for link in onward({"z": z, "y": y}, first, second, half):
            queues[link].append((0 if link[0] == first else 1, slot, unit))

    for half in (0, 1):
        for matrix in (0, 1):
            offer((matrix, 0, 0, half), 0)
    slots, landed = [], {}
    while any(queues.values()) or any(landed.values()):
        now = len(slots)
        for unit in landed.pop(now - 2, []):
            offer(unit, now)
        leaving = []
        for link in links:
            if queues[link]:
                choice = min(queues[link], key=lambda entry: entry[:2])
                queues[link].remove(choice)
                leaving.append((link, choice[2]))
        landed[now] = []
        for (axis, sign), (matrix, z, y, half) in leaving:
            landed[now].append((matrix, z + sign * (axis == "z"), y + sign * (axis == "y"), half))
        slots.append(leaving)
        if len(slots) > 100:
            raise ValueError("plan")
    while slots and not slots[-1]:
        slots.pop()
    return slots


def token_plan(pieces):
    own = {1: list(range(pieces)), -1: list(range(pieces))}
    passing = {1: [], -1: []}
    slots, landed = [], {}
    while own[1] or own[-1] or passing[1] or passing[-1] or any(landed.values()):
        now = len(slots)
        for sign, hops, piece in landed.pop(now - 2, []):
            if hops == 1 and (piece % 2 == 0) == (sign == 1):
                passing[sign].append(piece)
        leaving = []
        for sign in (1, -1):
            if passing[sign]:
                leaving.append((sign, 1, passing[sign].pop(0)))
            elif own[sign]:
                leaving.append((sign, 0, own[sign].pop(0)))
        landed[now] = [(sign, hops + 1, piece) for sign, hops, piece in leaving]
        slots.append(leaving)
    while slots and not slots[-1]:
        slots.pop()
    return slots


def place():
    fs, x = lax.axis_index("fs"), lax.axis_index("tp")
    core, chip = lax.rem(fs, 2), fs // 2
    return chip // RING, lax.rem(chip, RING), core, x


def turn(i, by):
    return lax.rem(i + by + 2 * RING, RING)


def gather_kernel(
    weights, token_slots, tok_ref, gain_in, up_in, down_in, up_ref, down_ref, all_ref,
    gain_ref, up_own, down_own, w_recv, t_recv, w_send, t_send, p_send, p_recv, own_sem,
):
    z, y, core, x = place()
    loads = [
        pltpu.make_async_copy(src, dst, own_sem.at[i])
        for i, (src, dst) in enumerate(
            ((gain_in, gain_ref), (up_in, up_own), (down_in, down_own), (tok_ref, all_ref.at[x]))
        )
    ]
    for load in loads:
        load.start()

    def device(dz=0, dy=0, dx=0, other=False):
        fs = (turn(z, dz) * RING + turn(y, dy)) * 2 + (1 - core if other else core)
        return (fs, turn(x, dx))

    barrier = pltpu.get_barrier_semaphore()
    neighbours = [device(other=True)] + [
        device(**{axis: sign}) for axis in ("dz", "dy", "dx") for sign in (1, -1)
    ]
    for neighbour in neighbours:
        pl.semaphore_signal(barrier, inc=1, device_id=neighbour, device_id_type=MESH)

    rows = up_in.shape[0]
    mine = pl.ds(pl.multiple_of(((z * RING + y) * 2 + core) * rows, rows), rows)
    square = (rows, rows)
    diagonal = lax.broadcasted_iota(jnp.int32, square, 0) == lax.broadcasted_iota(jnp.int32, square, 1)
    for load in loads[:3]:
        load.wait()
    gain = jnp.sum(jnp.where(diagonal, jnp.broadcast_to(gain_ref[...], square), 0.0), axis=1, keepdims=True)
    up_ref[mine, :] = (gain * up_own[...]).astype(BF16)
    down_ref[mine, :] = down_own[...].astype(BF16)
    pl.semaphore_wait(barrier, len(neighbours))

    tables = (up_ref, down_ref)

    def weight_rows(unit):
        matrix, hz, hy, half = unit
        source = (turn(z, -hz) * RING + turn(y, -hy)) * 2 + core
        start = pl.multiple_of(source * rows + half * HALF, HALF)
        return tables[matrix].at[pl.ds(start, HALF), :]

    def weight_copy(index, link, unit):
        ref = weight_rows(unit)
        to = device(**{"d" + link[0]: link[1]})
        return pltpu.make_async_remote_copy(ref, ref, w_send, w_recv.at[index], to, MESH)

    def partner_copy(unit):
        ref = weight_rows(unit)
        return pltpu.make_async_remote_copy(ref, ref, p_send, p_recv.at[unit[0]], device(other=True), MESH)

    def token_copy(index, sign, hops, piece):
        at = pl.ds(piece * PIECE, PIECE)
        there = all_ref.at[turn(x, -sign * hops), at, :]
        here = tok_ref.at[at, :] if hops == 0 else there
        return pltpu.make_async_remote_copy(here, there, t_send, t_recv.at[index], device(dx=sign), MESH)

    w_index = {}
    for leaving in weights:
        for entry in leaving:
            w_index[entry] = len(w_index)
    t_index = {}
    for leaving in token_slots:
        for entry in leaving:
            t_index[entry] = len(t_index)

    def send(slot):
        if slot < len(weights):
            for link, unit in weights[slot]:
                weight_copy(w_index[link, unit], link, unit).start()
        if slot < len(token_slots):
            for entry in token_slots[slot]:
                token_copy(t_index[entry], *entry).start()

    def receive(slot):
        if slot < len(weights):
            for link, unit in weights[slot]:
                matrix, hz, hy, half = unit
                got = (matrix, hz + link[1] * (link[0] == "z"), hy + link[1] * (link[0] == "y"), half)
                ref = weight_rows(got)
                pltpu.make_async_remote_copy(
                    ref, ref, w_send, w_recv.at[w_index[link, unit]], device(other=True), MESH
                ).wait_recv()
                partner_copy(got).start()
        if slot < len(token_slots):
            for sign, hops, piece in token_slots[slot]:
                at = pl.ds(piece * PIECE, PIECE)
                ref = all_ref.at[turn(x, -sign * (hops + 1)), at, :]
                pltpu.make_async_remote_copy(
                    ref, ref, t_send, t_recv.at[t_index[sign, hops, piece]], device(other=True), MESH
                ).wait_recv()

    last = max(len(weights), len(token_slots))
    send(0)
    for matrix in (0, 1):
        for half in (0, 1):
            partner_copy((matrix, 0, 0, half)).start()
    send(1)
    for slot in range(last):
        receive(slot)
        send(slot + 2)

    def settle(ref, sem):
        pltpu.make_async_copy(ref, ref, sem).wait()

    loads[3].wait()
    half_rows = up_ref.shape[0] // 2
    for matrix in (0, 1):
        settle(tables[matrix].at[pl.ds(0, half_rows), :], p_recv.at[matrix])
    for matrix in (0, 1):
        settle(tables[matrix].at[pl.ds(0, half_rows), :], p_send)
        settle(tables[matrix].at[pl.ds(0, len(w_index) // 2 * HALF), :], w_send)
    for _ in range(len(t_index) * PIECE // all_ref.shape[1]):
        settle(all_ref.at[0], t_send)


def apply_kernel(
    up_ref, down_ref, all_ref, out_ref,
    hidden_ref, far_ref, right_ref, left_ref, mine_ref, far_left, far_right, from_left, from_right,
    send_sem, far_recv, near_recv,
):
    z, y, core, x = place()
    fs = (z * RING + y) * 2 + core
    right, left = (fs, turn(x, 1)), (fs, turn(x, -1))
    barrier = pltpu.get_barrier_semaphore()
    for neighbour in (right, left):
        pl.semaphore_signal(barrier, inc=1, device_id=neighbour, device_id_type=MESH)

    sources, tokens, width = all_ref.shape
    features, units = up_ref.shape
    steps, half = tokens // CHUNK, CHUNK // 2
    tile = 512

    def span(step, part=None):
        if part is None:
            return pl.ds(pl.multiple_of(step * CHUNK, CHUNK), CHUNK)
        return pl.ds(pl.multiple_of(step * CHUNK + part * half, half), half)

    def packed(step):
        return pl.ds(pl.multiple_of(step * half, half), half)

    def far_copy(step, part):
        to, dst = (right, far_left) if part == 0 else (left, far_right)
        return pltpu.make_async_remote_copy(
            far_ref.at[span(step, part), :], dst.at[packed(step), :], send_sem, far_recv.at[step, part], to, MESH
        )

    def near_copy(step, side, part):
        to, src, dst = (right, right_ref, from_left) if side == 0 else (left, left_ref, from_right)
        return pltpu.make_async_remote_copy(
            src.at[span(step, part), :], dst.at[span(step, part), :], send_sem, near_recv.at[step, side, part], to, MESH
        )

    def compute(step):
        at = span(step)
        pieces = [all_ref[k, at, :].astype(F32) for k in range(sources)]
        total = sum(jnp.sum(p * p, axis=-1, keepdims=True) for p in pieces)
        scale = lax.rsqrt(total * (1.0 / features) + epsilon)
        normed = [(p * scale).astype(BF16) for p in pieces]
        for t in range(units // tile):
            cols = pl.ds(t * tile, tile)
            acc = jnp.zeros((CHUNK, tile), F32)
            for k in range(sources):
                acc += jnp.dot(normed[k], up_ref[pl.ds(k * width, width), cols], preferred_element_type=F32)
            hidden_ref[:, cols] = jnp.square(jnp.maximum(acc, 0.0)).astype(BF16)

        def block(by):
            cols = pl.ds(pl.multiple_of(turn(x, by) * width, width), width)
            return lax.dot_general(
                hidden_ref[...], down_ref[cols, :], (((1,), (1,)), ((), ())), preferred_element_type=F32
            ).astype(BF16)

        far_ref[at, :] = block(2)
        return block

    def rest(step, block):
        at = span(step)
        right_ref[at, :] = block(1)
        left_ref[at, :] = block(-1)
        mine_ref[at, :] = block(0)

    def pass_on(step):
        for part, buf, got in ((0, right_ref, far_left), (1, left_ref, far_right)):
            far_copy(step, part).wait_recv()
            at = span(step, part)
            buf[at, :] = (buf[at, :].astype(F32) + got[packed(step), :].astype(F32)).astype(BF16)
            near_copy(step, part, part).start()

    def one_step(step, first):
        block = compute(step)
        if first:
            pl.semaphore_wait(barrier, 2)
        for part in (0, 1):
            far_copy(step, part).start()
        rest(step, block)
        near_copy(step, 0, 1).start()
        near_copy(step, 1, 0).start()

    one_step(0, True)

    def body(step, carry):
        one_step(step, False)
        pass_on(step - 1)
        return carry

    lax.fori_loop(1, steps, body, 0)
    pass_on(steps - 1)

    def finish(step, carry):
        for part in (0, 1):
            for side in (0, 1):
                near_copy(step, side, part).wait_recv()
        at = span(step)
        total = mine_ref[at, :].astype(F32) + from_left[at, :].astype(F32) + from_right[at, :].astype(F32)
        out_ref[at, :] = total.astype(BF16)
        return carry

    lax.fori_loop(0, steps, finish, 0)
    for buf in (far_ref, right_ref, left_ref):
        pltpu.make_async_copy(buf, buf, send_sem).wait()


def on_device(tokens, norm_gain, up_weight, down_weight):
    count, width = tokens.shape
    features, units = width * RING, up_weight.shape[1]
    weights, token_slots = weight_plan(), token_plan(count // PIECE)
    vmem = pl.BlockSpec(memory_space=pltpu.VMEM)
    dma = pltpu.SemaphoreType.DMA
    up, down, gathered = pl.pallas_call(
        functools.partial(gather_kernel, weights, token_slots),
        name="gather",
        out_shape=(
            pltpu.VMEM((features, units), BF16),
            pltpu.VMEM((features, units), BF16),
            pltpu.VMEM((RING, count, width), BF16),
        ),
        in_specs=[pl.BlockSpec(memory_space=pltpu.HBM)] * 4,
        out_specs=(vmem, vmem, vmem),
        scratch_shapes=[
            pltpu.VMEM((1, norm_gain.shape[0]), F32), pltpu.VMEM(up_weight.shape, F32), pltpu.VMEM(up_weight.shape, F32),
            dma((sum(map(len, weights)),)), dma((sum(map(len, token_slots)),)), dma, dma, dma, dma((2,)), dma((4,)),
        ],
        compiler_params=pltpu.CompilerParams(collective_id=0, has_side_effects=True, vmem_limit_bytes=36 * 2**20),
    )(tokens, norm_gain[None, :], up_weight, down_weight)
    steps = count // CHUNK
    rows = pltpu.VMEM((count, width), BF16)
    half_rows = pltpu.VMEM((count // 2, width), BF16)
    mixed = pl.pallas_call(
        apply_kernel,
        name="apply",
        out_shape=pltpu.VMEM((count, width), BF16),
        in_specs=[vmem, vmem, vmem],
        out_specs=vmem,
        scratch_shapes=[
            pltpu.VMEM((CHUNK, units), BF16), rows, rows, rows, rows, half_rows, half_rows, rows, rows,
            dma, dma((steps, 2)), dma((steps, 2, 2)),
        ],
        compiler_params=pltpu.CompilerParams(collective_id=1, has_side_effects=True, vmem_limit_bytes=30 * 2**20),
    )(up, down, gathered)
    return up, down, mixed


def solution(mesh):
    return jax.shard_map(
        on_device,
        mesh=mesh,
        in_specs=(P("fs", "tp"), P("fs"), P("fs", "tp"), P("fs", "tp")),
        out_specs=(P(None, "tp"), P(None, "tp"), P("fs", "tp")),
        check_vma=False,
    )
```

time: 212 us -> 128 us (0.60); the launches traced: 212 us -> 125 us
  Pallas kernels: 0 us -> 117 us
  blocking collectives: 75 us -> 0 us
  waiting for transfers between devices: 65.7 us -> 0 us
  matrix products: 34.5 us -> 0 us
  between operations: 14.1 us -> 0.65 us
  other arithmetic: 8.33 us -> 0 us
  local copies, waits for them, and re-layouts: 14.1 us -> 7.94 us
    pallas_call x0 -> x2, Pallas kernels: none -> 117 us  [the longest x1 58.9 us: on_device(): pl.pallas_call(functools.partial(gather_kernel, weights, token_slots), na...]
    all_to_all x1 -> x0, blocking collectives: 75 us -> none  [sent_to_all(): lax.all_to_all(jnp.broadcast_to(x[None], (devices, *x.shape)), axis, 0, 0...]
    reduce_scatter x1 -> x0, waiting for transfers between devices: 65.7 us -> none  [on_device(): lax.psum_scatter(rounded.astype(jnp.bfloat16), 'tp', scatter_dimension=1,...]
    dot_general x1 -> x0, matrix products: 34.5 us -> none  [on_device(): lax.dot_general(hidden, down_matrix, (((1,), (1,)), ((), ())), preferred_...]
    slice x1 -> x0, local copies, waits for them, and re-layouts: 11.9 us -> none  [side_by_side(): lax.slice_in_dim(filled, at, at + a.shape[along], axis=along)]
    unnamed x1 -> x3, local copies, waits for them, and re-layouts: 1.72 us -> 7.94 us
    convert_element_type x3 -> x0, other arithmetic: 6.19 us -> none  [the longest x1 3.98 us: row_scale(): return scaled.astype(jnp.bfloat16)]
  transfers between devices with their start and end apart: 2 -> 0, of which waited for: 1 -> 0; matrix products, arithmetic and copies ran while one was open for 4% -> 0% of each run, Pallas kernels for 0% -> 0%
where the time goes in v1:
time: 128 us; the launch traced here: 125 us
  Pallas kernels  117 us (91%)
  local copies, waits for them, and re-layouts  7.94 us (6%)
    pallas_call x1, Pallas kernels, on_device(): pl.pallas_call(functools.partial(gather_kernel, weights, token_slots), na...  58.9 us
    pallas_call x1, Pallas kernels, on_device(): pl.pallas_call(apply_kernel, name='apply', out_shape=pltpu.VMEM((count, w...  57.7 us
    unnamed x3, local copies, waits for them, and re-layouts  7.94 us

profile of v1, /device:TPU:1, one launch (start us, length us, event | category | flops | bytes accessed | tf_op | source)
XLA Modules:
  0.0 125.2 jit_solution(2395791491787495955)
XLA Ops:
  0.6 58.9 %gather.1 = (bf16[2048,2048]{1,0:T(8,128)(2,1)S(1)}, bf16[2048,2048]{1,0:T(8,128)(2,1)S(1)}, bf16[4,1536,512]{2,1,0:T(8,128)(2,1)S(1)}) custom-call(bf16[1536,512]{1,0:T(8,128)(2,1)} %tok_ref.1, f32[1,64]{1,0:T(1,128)} %bitcast.1, f32[64,2048]{1,0:T(8,128)} %up_in.1, f32[64,2048]{1,0:T(8,128)} %down_in.1), custom_call_target="tpu_custom_call" | custom-call | tf_op jit(solution)/shard_map/gather/pallas_call | solution.py:333
  59.5 57.7 %apply.1 = bf16[1536,512]{1,0:T(8,128)(2,1)S(1)} custom-call(bf16[2048,2048]{1,0:T(8,128)(2,1)S(1)} %get-tuple-element.9.up_ref, bf16[2048,2048]{1,0:T(8,128)(2,1)S(1)} %get-tuple-element.10.down_ref, bf16[4,1536,512]{2,1,0:T(8,128)(2,1)S(1)} %get-tuple-element.8.all_ref), custom_call_target="tpu_custom_call" | custom-call | tf_op jit(solution)/shard_map/apply/pallas_call | solution.py:352
  117.2 3.4 %copy.11 = bf16[2048,2048]{1,0:T(8,128)(2,1)} copy(bf16[2048,2048]{1,0:T(8,128)(2,1)S(1)} %get-tuple-element.10.down_ref) | data formatting | bytes 16777216
  120.6 3.4 %copy.10 = bf16[2048,2048]{1,0:T(8,128)(2,1)} copy(bf16[2048,2048]{1,0:T(8,128)(2,1)S(1)} %get-tuple-element.9.up_ref) | data formatting | bytes 16777216
  124.0 1.1 copy.12

commit v2 on v1

--- a/solution.py
+++ b/solution.py
@@ -11,6 +11,7 @@
 RING = 4
 HALF = 32
 PIECE = 128
+LAG = 3
 CHUNK = 256
 MESH = pl.DeviceIdType.MESH
 F32, BF16 = jnp.float32, jnp.bfloat16
@@ -49,7 +50,7 @@
     slots, landed = [], {}
     while any(queues.values()) or any(landed.values()):
         now = len(slots)
-        for unit in landed.pop(now - 2, []):
+        for unit in landed.pop(now - LAG, []):
             offer(unit, now)
         leaving = []
         for link in links:
@@ -74,7 +75,7 @@
     slots, landed = [], {}
     while own[1] or own[-1] or passing[1] or passing[-1] or any(landed.values()):
         now = len(slots)
-        for sign, hops, piece in landed.pop(now - 2, []):
+        for sign, hops, piece in landed.pop(now - LAG, []):
             if hops == 1 and (piece % 2 == 0) == (sign == 1):
                 passing[sign].append(piece)
         leaving = []
@@ -100,9 +101,11 @@
     return lax.rem(i + by + 2 * RING, RING)
 
 
-def gather_kernel(
-    weights, token_slots, tok_ref, gain_in, up_in, down_in, up_ref, down_ref, all_ref,
-    gain_ref, up_own, down_own, w_recv, t_recv, w_send, t_send, p_send, p_recv, own_sem,
+def layer_kernel(
+    weights, token_slots, tok_ref, gain_in, up_in, down_in, up_ref, down_ref, out_ref,
+    gain_ref, up_own, down_own, all_ref,
+    hidden_ref, far_ref, right_ref, left_ref, mine_ref, far_left, far_right, from_left, from_right,
+    w_recv, t_recv, w_send, t_send, p_send, p_recv, own_sem, send_sem, far_recv, near_recv,
 ):
     z, y, core, x = place()
     loads = [
@@ -126,16 +129,6 @@
         pl.semaphore_signal(barrier, inc=1, device_id=neighbour, device_id_type=MESH)
 
     rows = up_in.shape[0]
-    mine = pl.ds(pl.multiple_of(((z * RING + y) * 2 + core) * rows, rows), rows)
-    square = (rows, rows)
-    diagonal = lax.broadcasted_iota(jnp.int32, square, 0) == lax.broadcasted_iota(jnp.int32, square, 1)
-    for load in loads[:3]:
-        load.wait()
-    gain = jnp.sum(jnp.where(diagonal, jnp.broadcast_to(gain_ref[...], square), 0.0), axis=1, keepdims=True)
-    up_ref[mine, :] = (gain * up_own[...]).astype(BF16)
-    down_ref[mine, :] = down_own[...].astype(BF16)
-    pl.semaphore_wait(barrier, len(neighbours))
-
     tables = (up_ref, down_ref)
 
     def weight_rows(unit):
@@ -168,15 +161,17 @@
         for entry in leaving:
             t_index[entry] = len(t_index)
 
-    def send(slot):
+    def send_weights(slot):
         if slot < len(weights):
             for link, unit in weights[slot]:
                 weight_copy(w_index[link, unit], link, unit).start()
+
+    def send_tokens(slot):
         if slot < len(token_slots):
             for entry in token_slots[slot]:
                 token_copy(t_index[entry], *entry).start()
 
-    def receive(slot):
+    def receive_weights(slot):
         if slot < len(weights):
             for link, unit in weights[slot]:
                 matrix, hz, hy, half = unit
@@ -186,23 +181,37 @@
                     ref, ref, w_send, w_recv.at[w_index[link, unit]], device(other=True), MESH
                 ).wait_recv()
                 partner_copy(got).start()
-        if slot < len(token_slots):
-            for sign, hops, piece in token_slots[slot]:
-                at = pl.ds(piece * PIECE, PIECE)
-                ref = all_ref.at[turn(x, -sign * (hops + 1)), at, :]
-                pltpu.make_async_remote_copy(
-                    ref, ref, t_send, t_recv.at[t_index[sign, hops, piece]], device(other=True), MESH
-                ).wait_recv()
-
-    last = max(len(weights), len(token_slots))
-    send(0)
+
+    def receive_tokens(slot):
+        for sign, hops, piece in token_slots[slot]:
+            at = pl.ds(piece * PIECE, PIECE)
+            ref = all_ref.at[turn(x, -sign * (hops + 1)), at, :]
+            pltpu.make_async_remote_copy(
+                ref, ref, t_send, t_recv.at[t_index[sign, hops, piece]], device(other=True), MESH
+            ).wait_recv()
+
+    pl.semaphore_wait(barrier, len(neighbours))
+    for slot in range(LAG):
+        send_tokens(slot)
+    mine = pl.ds(pl.multiple_of(((z * RING + y) * 2 + core) * rows, rows), rows)
+    square = (rows, rows)
+    diagonal = lax.broadcasted_iota(jnp.int32, square, 0) == lax.broadcasted_iota(jnp.int32, square, 1)
+    for load in loads[:3]:
+        load.wait()
+    gain = jnp.sum(jnp.where(diagonal, jnp.broadcast_to(gain_ref[...], square), 0.0), axis=1, keepdims=True)
+    up_ref[mine, :] = (gain * up_own[...]).astype(BF16)
+    down_ref[mine, :] = down_own[...].astype(BF16)
+    for slot in range(LAG):
+        send_weights(slot)
     for matrix in (0, 1):
         for half in (0, 1):
             partner_copy((matrix, 0, 0, half)).start()
-    send(1)
-    for slot in range(last):
-        receive(slot)
-        send(slot + 2)
+    early = len(weights)
+    for slot in range(early):
+        receive_weights(slot)
+        receive_tokens(slot)
+        send_weights(slot + LAG)
+        send_tokens(slot + LAG)
 
     def settle(ref, sem):
         pltpu.make_async_copy(ref, ref, sem).wait()
@@ -211,25 +220,8 @@
     half_rows = up_ref.shape[0] // 2
     for matrix in (0, 1):
         settle(tables[matrix].at[pl.ds(0, half_rows), :], p_recv.at[matrix])
-    for matrix in (0, 1):
-        settle(tables[matrix].at[pl.ds(0, half_rows), :], p_send)
-        settle(tables[matrix].at[pl.ds(0, len(w_index) // 2 * HALF), :], w_send)
-    for _ in range(len(t_index) * PIECE // all_ref.shape[1]):
-        settle(all_ref.at[0], t_send)
-
-
-def apply_kernel(
-    up_ref, down_ref, all_ref, out_ref,
-    hidden_ref, far_ref, right_ref, left_ref, mine_ref, far_left, far_right, from_left, from_right,
-    send_sem, far_recv, near_recv,
-):
-    z, y, core, x = place()
-    fs = (z * RING + y) * 2 + core
-    right, left = (fs, turn(x, 1)), (fs, turn(x, -1))
-    barrier = pltpu.get_barrier_semaphore()
-    for neighbour in (right, left):
-        pl.semaphore_signal(barrier, inc=1, device_id=neighbour, device_id_type=MESH)
-
+
+    right, left = device(dx=1), device(dx=-1)
     sources, tokens, width = all_ref.shape
     features, units = up_ref.shape
     steps, half = tokens // CHUNK, CHUNK // 2
@@ -290,20 +282,32 @@
             buf[at, :] = (buf[at, :].astype(F32) + got[packed(step), :].astype(F32)).astype(BF16)
             near_copy(step, part, part).start()
 
-    def one_step(step, first):
+    def one_step(step):
         block = compute(step)
-        if first:
-            pl.semaphore_wait(barrier, 2)
         for part in (0, 1):
             far_copy(step, part).start()
+        return block
+
+    def two_step(step, block):
         rest(step, block)
         near_copy(step, 0, 1).start()
         near_copy(step, 1, 0).start()
 
-    one_step(0, True)
+    block = one_step(0)
+    for slot in range(early, len(token_slots) - LAG):
+        receive_tokens(slot)
+        send_tokens(slot + LAG)
+    two_step(0, block)
+    late = range(max(early, len(token_slots) - LAG), len(token_slots))
+    needed = min(piece for slot in late for _, _, piece in token_slots[slot]) * PIECE // CHUNK
 
     def body(step, carry):
-        one_step(step, False)
+        @pl.when(step == needed)
+        def _():
+            for slot in late:
+                receive_tokens(slot)
+
+        two_step(step, one_step(step))
         pass_on(step - 1)
         return carry
 
@@ -322,46 +326,57 @@
     lax.fori_loop(0, steps, finish, 0)
     for buf in (far_ref, right_ref, left_ref):
         pltpu.make_async_copy(buf, buf, send_sem).wait()
+    for matrix in (0, 1):
+        settle(tables[matrix].at[pl.ds(0, half_rows), :], p_send)
+        settle(tables[matrix].at[pl.ds(0, len(w_index) // 2 * HALF), :], w_send)
+    for _ in range(len(t_index) * PIECE // all_ref.shape[1]):
+        settle(all_ref.at[0], t_send)
+
+
+def store_kernel(up_ref, down_ref, mixed_ref, up_out, down_out, mixed_out, sem):
+    copies = [
+        pltpu.make_async_copy(src, dst, sem.at[i])
+        for i, (src, dst) in enumerate(((up_ref, up_out), (down_ref, down_out), (mixed_ref, mixed_out)))
+    ]
+    for copy in copies:
+        copy.start()
+    for copy in copies:
+        copy.wait()
 
 
 def on_device(tokens, norm_gain, up_weight, down_weight):
     count, width = tokens.shape
     features, units = width * RING, up_weight.shape[1]
     weights, token_slots = weight_plan(), token_plan(count // PIECE)
-    vmem = pl.BlockSpec(memory_space=pltpu.VMEM)
+    steps = count // CHUNK
+    vmem, hbm = pl.BlockSpec(memory_space=pltpu.VMEM), pl.BlockSpec(memory_space=pltpu.HBM)
     dma = pltpu.SemaphoreType.DMA
-    up, down, gathered = pl.pallas_call(
-        functools.partial(gather_kernel, weights, token_slots),
-        name="gather",
-        out_shape=(
-            pltpu.VMEM((features, units), BF16),
-            pltpu.VMEM((features, units), BF16),
-            pltpu.VMEM((RING, count, width), BF16),
-        ),
-        in_specs=[pl.BlockSpec(memory_space=pltpu.HBM)] * 4,
-        out_specs=(vmem, vmem, vmem),
+    rows, half_rows = pltpu.VMEM((count, width), BF16), pltpu.VMEM((count // 2, width), BF16)
+    shapes = ((features, units), (features, units), (count, width))
+    results = pl.pallas_call(
+        functools.partial(layer_kernel, weights, token_slots),
+        name="layer",
+        out_shape=[pltpu.VMEM(shape, BF16) for shape in shapes],
+        in_specs=[hbm] * 4,
+        out_specs=[vmem] * 3,
         scratch_shapes=[
             pltpu.VMEM((1, norm_gain.shape[0]), F32), pltpu.VMEM(up_weight.shape, F32), pltpu.VMEM(up_weight.shape, F32),
+            pltpu.VMEM((RING, count, width), BF16),
+            pltpu.VMEM((CHUNK, units), BF16), rows, rows, rows, rows, half_rows, half_rows, rows, rows,
             dma((sum(map(len, weights)),)), dma((sum(map(len, token_slots)),)), dma, dma, dma, dma((2,)), dma((4,)),
-        ],
-        compiler_params=pltpu.CompilerParams(collective_id=0, has_side_effects=True, vmem_limit_bytes=36 * 2**20),
-    )(tokens, norm_gain[None, :], up_weight, down_weight)
-    steps = count // CHUNK
-    rows = pltpu.VMEM((count, width), BF16)
-    half_rows = pltpu.VMEM((count // 2, width), BF16)
-    mixed = pl.pallas_call(
-        apply_kernel,
-        name="apply",
-        out_shape=pltpu.VMEM((count, width), BF16),
-        in_specs=[vmem, vmem, vmem],
-        out_specs=vmem,
-        scratch_shapes=[
-            pltpu.VMEM((CHUNK, units), BF16), rows, rows, rows, rows, half_rows, half_rows, rows, rows,
             dma, dma((steps, 2)), dma((steps, 2, 2)),
         ],
-        compiler_params=pltpu.CompilerParams(collective_id=1, has_side_effects=True, vmem_limit_bytes=30 * 2**20),
-    )(up, down, gathered)
-    return up, down, mixed
+        compiler_params=pltpu.CompilerParams(collective_id=0, has_side_effects=True, vmem_limit_bytes=42 * 2**20),
+    )(tokens, norm_gain[None, :], up_weight, down_weight)
+    return pl.pallas_call(
+        store_kernel,
+        name="store",
+        out_shape=[jax.ShapeDtypeStruct(shape, BF16) for shape in shapes],
+        in_specs=[vmem] * 3,
+        out_specs=[hbm] * 3,
+        scratch_shapes=[dma((3,))],
+        compiler_params=pltpu.CompilerParams(vmem_limit_bytes=2**20),
+    )(*results)
 
 
 def solution(mesh):

time: 128 us -> 119 us (0.930); the launches traced: 125 us -> 119 us
  local copies, waits for them, and re-layouts: 7.94 us -> 0 us
    unnamed x3 -> x0, local copies, waits for them, and re-layouts: 7.94 us -> none
    pallas_call x2, Pallas kernels: 117 us -> 118 us  [the longest x1 112 us: on_device(): pl.pallas_call(functools.partial(layer_kernel, weights, token_slots), nam...]
where the time goes in v2:
time: 119 us
  Pallas kernels  118 us (99%)
    pallas_call x1, Pallas kernels, on_device(): pl.pallas_call(functools.partial(layer_kernel, weights, token_slots), nam...  112 us
    pallas_call x1, Pallas kernels, on_device(): pl.pallas_call(store_kernel, name='store', out_shape=[jax.ShapeDtypeStruc...  6.45 us

profile of v2, /device:TPU:1, one launch (start us, length us, event | category | flops | bytes accessed | tf_op | source)
XLA Modules:
  0.0 119.0 jit_solution(12985818536929871847)
XLA Ops:
  0.6 111.9 %layer.1 = (bf16[2048,2048]{1,0:T(8,128)(2,1)S(1)}, bf16[2048,2048]{1,0:T(8,128)(2,1)S(1)}, bf16[1536,512]{1,0:T(8,128)(2,1)S(1)}) custom-call(bf16[1536,512]{1,0:T(8,128)(2,1)} %tok_ref.1, f32[1,64]{1,0:T(1,128)} %bitcast.1, f32[64,2048]{1,0:T(8,128)} %up_in.1, f32[64,2048]{1,0:T(8,128)} %down_in.1), custom_call_target="tpu_custom_call" | custom-call | tf_op jit(solution)/shard_map/layer/pallas_call | solution.py:356
  112.5 6.5 %store.1 = (bf16[2048,2048]{1,0:T(8,128)(2,1)}, bf16[2048,2048]{1,0:T(8,128)(2,1)}, bf16[1536,512]{1,0:T(8,128)(2,1)}) custom-call(bf16[2048,2048]{1,0:T(8,128)(2,1)S(1)} %get-tuple-element.6.up_ref, bf16[2048,2048]{1,0:T(8,128)(2,1)S(1)} %get-tuple-element.7.down_ref, bf16[1536,512]{1,0:T(8,128)(2,1)S(1)} %get-tuple-element.8.mixed_ref), custom_call_target="tpu_custom_call" | custom-call | tf_op jit(solution)/shard_map/store/pallas_call | solution.py:371

commit v3 on v1

v3 whole, which is shorter than its diff:
```python
import functools

import jax
import jax.numpy as jnp
from jax import lax
from jax.experimental import pallas as pl
from jax.experimental.pallas import tpu as pltpu
from jax.sharding import PartitionSpec as P

epsilon = 1e-06
RING = 4
HALF = 32
PIECE = 128
LAG = 3
TOKEN_LAG = 6
TURN = 2
PACE = {0: (2,) * 3 + (1,) * 12, 1: (0,) * 3 + (1,) * 12}
CHUNK = 256
MESH = pl.DeviceIdType.MESH
F32, BF16 = jnp.float32, jnp.bfloat16


def onward(at, first, second, half):
    links = []
    if at[second] == 0:
        if at[first] == 0:
            links += [(first, 1), (first, -1)]
        elif at[first] == 1 and half == 0:
            links += [(first, 1)]
        elif at[first] == -1 and half == 1:
            links += [(first, -1)]
        links += [(second, 1), (second, -1)]
    elif at[second] == 1 and half == 0:
        links += [(second, 1)]
    elif at[second] == -1 and half == 1:
        links += [(second, -1)]
    return links


def weight_plan():
    links = [(axis, sign) for axis in "yz" for sign in (1, -1)]
    queues = {link: [] for link in links}

    def offer(unit, slot):
        matrix, z, y, half = unit
        first, second = ("y", "z") if matrix == 0 else ("z", "y")
        for link in onward({"z": z, "y": y}, first, second, half):
            queues[link].append((0 if link[0] == first else 1, slot, unit))

    for half in (0, 1):
        for matrix in (0, 1):
            offer((matrix, 0, 0, half), 0)
    slots, landed = [], {}
    while any(queues.values()) or any(landed.values()):
        now = len(slots)
        for unit in landed.pop(now - LAG, []):
            offer(unit, now)
        leaving = []
        for link in links:
            if queues[link]:
                choice = min(queues[link], key=lambda entry: entry[:2])
                queues[link].remove(choice)
                leaving.append((link, choice[2]))
        landed[now] = []
        for (axis, sign), (matrix, z, y, half) in leaving:
            landed[now].append((matrix, z + sign * (axis == "z"), y + sign * (axis == "y"), half))
        slots.append(leaving)
        if len(slots) > 100:
            raise ValueError("plan")
    while slots and not slots[-1]:
        slots.pop()
    return slots


def token_plan(pieces):
    evens, odds = list(range(0, pieces, 2)), list(range(1, pieces, 2))
    own = {1: evens + odds, -1: odds + evens}
    passing = {1: [], -1: []}
    slots, landed = [], {}
    while own[1] or own[-1] or passing[1] or passing[-1] or any(landed.values()):
        now = len(slots)
        for sign, hops, piece in landed.pop(now - TOKEN_LAG, []):
            if hops == 1 and (piece % 2 == 0) == (sign == 1):
                passing[sign].append(piece)
        leaving = []
        for sign in (1, -1):
            if passing[sign]:
                leaving.append((sign, 1, passing[sign].pop(0)))
            elif own[sign]:
                leaving.append((sign, 0, own[sign].pop(0)))
        landed[now] = [(sign, hops + 1, piece) for sign, hops, piece in leaving]
        slots.append(leaving)
    while slots and not slots[-1]:
        slots.pop()
    return slots


def place():
    fs, x = lax.axis_index("fs"), lax.axis_index("tp")
    core, chip = lax.rem(fs, 2), fs // 2
    return chip // RING, lax.rem(chip, RING), core, x


def turn(i, by):
    return lax.rem(i + by + 2 * RING, RING)


def gather_kernel(
    weights, token_slots, tok_ref, gain_in, up_in, down_in, up_ref, down_ref, all_ref,
    gain_ref, up_own, down_own, w_recv, t_recv, w_send, t_send, p_send, p_recv, own_sem,
):
    z, y, core, x = place()
    loads = [
        pltpu.make_async_copy(src, dst, own_sem.at[i])
        for i, (src, dst) in enumerate(
            ((gain_in, gain_ref), (up_in, up_own), (down_in, down_own), (tok_ref, all_ref.at[x]))
        )
    ]
    for load in loads:
        load.start()

    def device(dz=0, dy=0, dx=0, other=False):
        fs = (turn(z, dz) * RING + turn(y, dy)) * 2 + (1 - core if other else core)
        return (fs, turn(x, dx))

    barrier = pltpu.get_barrier_semaphore()
    neighbours = [device(other=True)] + [
        device(**{axis: sign}) for axis in ("dz", "dy", "dx") for sign in (1, -1)
    ]
    for neighbour in neighbours:
        pl.semaphore_signal(barrier, inc=1, device_id=neighbour, device_id_type=MESH)

    rows = up_in.shape[0]
    tables = (up_ref, down_ref)

    def weight_rows(unit):
        matrix, hz, hy, half = unit
        source = (turn(z, -hz) * RING + turn(y, -hy)) * 2 + core
        start = pl.multiple_of(source * rows + half * HALF, HALF)
        return tables[matrix].at[pl.ds(start, HALF), :]

    def weight_copy(index, link, unit):
        ref = weight_rows(unit)
        to = device(**{"d" + link[0]: link[1]})
        return pltpu.make_async_remote_copy(ref, ref, w_send, w_recv.at[index], to, MESH)

    def partner_copy(unit):
        ref = weight_rows(unit)
        return pltpu.make_async_remote_copy(ref, ref, p_send, p_recv.at[unit[0]], device(other=True), MESH)

    def token_copy(index, sign, hops, piece):
        at = pl.ds(piece * PIECE, PIECE)
        there = all_ref.at[turn(x, -sign * hops), at, :]
        here = tok_ref.at[at, :] if hops == 0 else there
        return pltpu.make_async_remote_copy(here, there, t_send, t_recv.at[index], device(dx=sign), MESH)

    w_index = {}
    for leaving in weights:
        for entry in leaving:
            w_index[entry] = len(w_index)
    t_index = {}
    for leaving in token_slots:
        for entry in leaving:
            t_index[entry] = len(t_index)

    def send_weights(slot):
        if slot < len(weights):
            for link, unit in weights[slot]:
                weight_copy(w_index[link, unit], link, unit).start()

    def send_tokens(slot):
        if slot < len(token_slots):
            for entry in token_slots[slot]:
                token_copy(t_index[entry], *entry).start()

    def receive_weights(slot):
        for link, unit in weights[slot]:
            matrix, hz, hy, half = unit
            got = (matrix, hz + link[1] * (link[0] == "z"), hy + link[1] * (link[0] == "y"), half)
            ref = weight_rows(got)
            pltpu.make_async_remote_copy(
                ref, ref, w_send, w_recv.at[w_index[link, unit]], device(other=True), MESH
            ).wait_recv()
            partner_copy(got).start()

    def receive_tokens(slot):
        for sign, hops, piece in token_slots[slot]:
            at = pl.ds(piece * PIECE, PIECE)
            ref = all_ref.at[turn(x, -sign * (hops + 1)), at, :]
            pltpu.make_async_remote_copy(
                ref, ref, t_send, t_recv.at[t_index[sign, hops, piece]], device(other=True), MESH
            ).wait_recv()

    def first_tokens():
        for slot in range(TOKEN_LAG):
            send_tokens(slot)

    def next_tokens(slot):
        if slot < len(token_slots):
            receive_tokens(slot)
            send_tokens(slot + TOKEN_LAG)

    pl.semaphore_wait(barrier, len(neighbours))

    @pl.when(core == 0)
    def _():
        first_tokens()

    mine = pl.ds(pl.multiple_of(((z * RING + y) * 2 + core) * rows, rows), rows)
    square = (rows, rows)
    diagonal = lax.broadcasted_iota(jnp.int32, square, 0) == lax.broadcasted_iota(jnp.int32, square, 1)
    for load in loads[:3]:
        load.wait()
    gain = jnp.sum(jnp.where(diagonal, jnp.broadcast_to(gain_ref[...], square), 0.0), axis=1, keepdims=True)
    up_ref[mine, :] = (gain * up_own[...]).astype(BF16)
    down_ref[mine, :] = down_own[...].astype(BF16)
    for slot in range(LAG):
        send_weights(slot)
    for matrix in (0, 1):
        for half in (0, 1):
            partner_copy((matrix, 0, 0, half)).start()
    done = {0: 0, 1: 0}
    for slot in range(len(weights)):
        receive_weights(slot)
        send_weights(slot + LAG)
        for which in (0, 1):
            steps = range(done[which], min(done[which] + PACE[which][slot], len(token_slots)))
            done[which] = max(done[which], steps.stop)
            if steps or (which == 1 and slot == TURN):

                @pl.when(core == which)
                def _(slot=slot, which=which, steps=steps):
                    if which == 1 and slot == TURN:
                        first_tokens()
                    for step in steps:
                        next_tokens(step)

    for which in (0, 1):

        @pl.when(core == which)
        def _(which=which):
            for step in range(done[which], len(token_slots)):
                next_tokens(step)

    def settle(ref, sem):
        pltpu.make_async_copy(ref, ref, sem).wait()

    loads[3].wait()
    half_rows = up_ref.shape[0] // 2
    for matrix in (0, 1):
        settle(tables[matrix].at[pl.ds(0, half_rows), :], p_recv.at[matrix])
    for matrix in (0, 1):
        settle(tables[matrix].at[pl.ds(0, half_rows), :], p_send)
        settle(tables[matrix].at[pl.ds(0, len(w_index) // 2 * HALF), :], w_send)
    for _ in range(len(t_index) * PIECE // all_ref.shape[1]):
        settle(all_ref.at[0], t_send)


def products(x, all_ref, up_ref, down_ref, hidden_ref, at):
    sources, _, width = all_ref.shape
    features, units = up_ref.shape
    tile = 512
    pieces = [all_ref[k, at, :].astype(F32) for k in range(sources)]
    total = sum(jnp.sum(p * p, axis=-1, keepdims=True) for p in pieces)
    scale = lax.rsqrt(total * (1.0 / features) + epsilon)
    normed = [(p * scale).astype(BF16) for p in pieces]
    for t in range(units // tile):
        cols = pl.ds(t * tile, tile)
        acc = jnp.zeros((CHUNK, tile), F32)
        for k in range(sources):
            acc += jnp.dot(normed[k], up_ref[pl.ds(k * width, width), cols], preferred_element_type=F32)
        hidden_ref[:, cols] = jnp.square(jnp.maximum(acc, 0.0)).astype(BF16)

    def block(by):
        cols = pl.ds(pl.multiple_of(turn(x, by) * width, width), width)
        return lax.dot_general(
            hidden_ref[...], down_ref[cols, :], (((1,), (1,)), ((), ())), preferred_element_type=F32
        ).astype(BF16)

    return block


TARGETS = (2, 1, -1, 0)


def store_kernel(which, up_ref, down_ref, *refs):
    *extra, up_out, down_out = refs[:-1] if len(refs) == 3 else (refs[0], *refs[3:5])
    sem = refs[-1]
    copies = []
    for m, (src, dst) in enumerate(((up_ref, up_out), (down_ref, down_out))):
        part = src.shape[0] // 4
        for i in range(4):
            at = pl.ds(i * part, part)
            copies.append(pltpu.make_async_copy(src.at[at, :], dst.at[at, :], sem.at[m * 4 + i]))

    if extra:
        more = pltpu.make_async_copy(extra[0], refs[5], sem.at[8])
        more.start()

    @pl.when(lax.rem(lax.axis_index("fs"), 2) == which)
    def _():
        for copy in copies:
            copy.start()
        for copy in copies:
            copy.wait()

    if extra:
        more.wait()


def apply_kernel(
    up_ref, down_ref, all_ref, stored_ref, out_ref,
    hidden_ref, far_ref, right_ref, left_ref, mine_ref, far_left, far_right, from_left, from_right,
    send_sem, far_recv, near_recv,
):
    z, y, core, x = place()
    fs = (z * RING + y) * 2 + core
    right, left = (fs, turn(x, 1)), (fs, turn(x, -1))
    barrier = pltpu.get_barrier_semaphore()
    for neighbour in (right, left):
        pl.semaphore_signal(barrier, inc=1, device_id=neighbour, device_id_type=MESH)

    tokens, width = out_ref.shape
    steps, half = tokens // CHUNK, CHUNK // 2

    def span(step, part=None):
        if part is None:
            return pl.ds(pl.multiple_of(step * CHUNK, CHUNK), CHUNK)
        return pl.ds(pl.multiple_of(step * CHUNK + part * half, half), half)

    def packed(step):
        return pl.ds(pl.multiple_of(step * half, half), half)

    def far_copy(step, part):
        to, dst = (right, far_left) if part == 0 else (left, far_right)
        return pltpu.make_async_remote_copy(
            far_ref.at[span(step, part), :], dst.at[packed(step), :], send_sem, far_recv.at[step, part], to, MESH
        )

    def near_copy(step, side, part):
        to, src, dst = (right, right_ref, from_left) if side == 0 else (left, left_ref, from_right)
        return pltpu.make_async_remote_copy(
            src.at[span(step, part), :], dst.at[span(step, part), :], send_sem, near_recv.at[step, side, part], to, MESH
        )

    def pass_on(step):
        for part, buf, got in ((0, right_ref, far_left), (1, left_ref, far_right)):
            far_copy(step, part).wait_recv()
            at = span(step, part)
            buf[at, :] = (buf[at, :].astype(F32) + got[packed(step), :].astype(F32)).astype(BF16)
            near_copy(step, part, part).start()

    partials = (far_ref, right_ref, left_ref, mine_ref)

    def send_far(step):
        for part in (0, 1):
            far_copy(step, part).start()

    def send_near(step):
        near_copy(step, 0, 1).start()
        near_copy(step, 1, 0).start()

    def multiply(step, first):
        at = span(step)
        block = products(x, all_ref, up_ref, down_ref, hidden_ref, at)
        far_ref[at, :] = block(TARGETS[0])
        if first:
            pl.semaphore_wait(barrier, 2)
        send_far(step)
        if not first:
            pass_on(step - 1)
        for buf, by in zip(partials[1:], TARGETS[1:]):
            buf[at, :] = block(by)
        send_near(step)

    multiply(0, True)

    def body(step, carry):
        multiply(step, False)
        return carry

    lax.fori_loop(1, steps, body, 0)
    pass_on(steps - 1)

    def finish(step, carry):
        for part in (0, 1):
            for side in (0, 1):
                near_copy(step, side, part).wait_recv()
        at = span(step)
        total = mine_ref[at, :].astype(F32) + from_left[at, :].astype(F32) + from_right[at, :].astype(F32)
        out_ref[at, :] = total.astype(BF16)
        return carry

    lax.fori_loop(0, steps, finish, 0)
    for buf in (far_ref, right_ref, left_ref):
        pltpu.make_async_copy(buf, buf, send_sem).wait()


def on_device(tokens, norm_gain, up_weight, down_weight):
    count, width = tokens.shape
    features, units = width * RING, up_weight.shape[1]
    weights, token_slots = weight_plan(), token_plan(count // PIECE)
    steps = count // CHUNK
    vmem, hbm = pl.BlockSpec(memory_space=pltpu.VMEM), pl.BlockSpec(memory_space=pltpu.HBM)
    dma = pltpu.SemaphoreType.DMA
    matrix = (features, units)
    hidden = pltpu.VMEM((CHUNK, units), BF16)
    up, down, gathered = pl.pallas_call(
        functools.partial(gather_kernel, weights, token_slots),
        name="gather",
        out_shape=[pltpu.VMEM(matrix, BF16), pltpu.VMEM(matrix, BF16), pltpu.VMEM((RING, count, width), BF16)],
        in_specs=[hbm] * 4,
        out_specs=[vmem] * 3,
        scratch_shapes=[
            pltpu.VMEM((1, norm_gain.shape[0]), F32), pltpu.VMEM(up_weight.shape, F32), pltpu.VMEM(up_weight.shape, F32),
            dma((sum(map(len, weights)),)), dma((sum(map(len, token_slots)),)), dma, dma, dma, dma((2,)), dma((4,)),
        ],
        compiler_params=pltpu.CompilerParams(collective_id=0, has_side_effects=True, vmem_limit_bytes=33 * 2**20),
    )(tokens, norm_gain[None, :], up_weight, down_weight)
    whole = jax.ShapeDtypeStruct(matrix, BF16)

    def pinned(*arrays):
        return [pltpu.with_memory_space_constraint(a, pltpu.VMEM) for a in arrays]

    stored = pl.pallas_call(
        functools.partial(store_kernel, 1),
        name="store",
        out_shape=[whole, whole],
        in_specs=[vmem] * 2,
        out_specs=[hbm] * 2,
        scratch_shapes=[dma((8,))],
        compiler_params=pltpu.CompilerParams(vmem_limit_bytes=8 * 2**20),
    )(*pinned(up, down))
    rows, half_rows = pltpu.VMEM((count, width), BF16), pltpu.VMEM((count // 2, width), BF16)
    mixed = pl.pallas_call(
        apply_kernel,
        name="apply",
        out_shape=pltpu.VMEM((count, width), BF16),
        in_specs=[vmem] * 3 + [hbm],
        out_specs=vmem,
        scratch_shapes=[
            hidden, rows, rows, rows, rows, half_rows, half_rows, rows, rows,
            dma, dma((steps, 2)), dma((steps, 2, 2)),
        ],
        compiler_params=pltpu.CompilerParams(collective_id=1, has_side_effects=True, vmem_limit_bytes=31 * 2**20),
    )(*pinned(up, down, gathered), stored[0])
    return pl.pallas_call(
        functools.partial(store_kernel, 0),
        name="finish",
        out_shape=[whole, whole, jax.ShapeDtypeStruct((count, width), BF16)],
        in_specs=[vmem] * 3 + [hbm] * 2,
        out_specs=[hbm] * 3,
        scratch_shapes=[dma((9,))],
        input_output_aliases={3: 0, 4: 1},
        compiler_params=pltpu.CompilerParams(vmem_limit_bytes=8 * 2**20),
    )(*pinned(up, down, mixed), *stored)


def solution(mesh):
    return jax.shard_map(
        on_device,
        mesh=mesh,
        in_specs=(P("fs", "tp"), P("fs"), P("fs", "tp"), P("fs", "tp")),
        out_specs=(P(None, "tp"), P(None, "tp"), P("fs", "tp")),
        check_vma=False,
    )
```

time: 128 us -> 117 us (0.914); the launches traced: 125 us -> 116 us
  local copies, waits for them, and re-layouts: 7.94 us -> 0 us
    pallas_call x1, Pallas kernels: 57.7 us -> 47.7 us  [on_device(): pl.pallas_call(apply_kernel, name='apply', out_shape=pltpu.VMEM((count, w...]
    unnamed x3 -> x0, local copies, waits for them, and re-layouts: 7.94 us -> none
    pallas_call x0 -> x2, Pallas kernels: none -> 7.16 us  [the longest x1 5.94 us: on_device(): pl.pallas_call(functools.partial(store_kernel, 1), name='store', out_shap...]
    pallas_call x1, Pallas kernels: 58.9 us -> 61 us  [on_device(): pl.pallas_call(functools.partial(gather_kernel, weights, token_slots), na...]
where the time goes in v3:
time: 117 us; the launch traced here: 116 us
  Pallas kernels  116 us (99%)
    pallas_call x1, Pallas kernels, on_device(): pl.pallas_call(functools.partial(gather_kernel, weights, token_slots), na...  61 us
    pallas_call x1, Pallas kernels, on_device(): pl.pallas_call(apply_kernel, name='apply', out_shape=pltpu.VMEM((count, w...  47.7 us
    pallas_call x1, Pallas kernels, on_device(): pl.pallas_call(functools.partial(store_kernel, 1), name='store', out_shap...  5.94 us

profile of v3, /device:TPU:1, one launch (start us, length us, event | category | flops | bytes accessed | tf_op | source)
XLA Modules:
  0.0 116.5 jit_solution(10677605577854179215)
XLA Ops:
  0.6 61.0 %gather.1 = (bf16[2048,2048]{1,0:T(8,128)(2,1)S(1)}, bf16[2048,2048]{1,0:T(8,128)(2,1)S(1)}, bf16[4,1536,512]{2,1,0:T(8,128)(2,1)S(1)}) custom-call(bf16[1536,512]{1,0:T(8,128)(2,1)} %tok_ref.1, f32[1,64]{1,0:T(1,128)} %bitcast.1, f32[64,2048]{1,0:T(8,128)} %up_in.1, f32[64,2048]{1,0:T(8,128)} %down_in.1), custom_call_target="tpu_custom_call" | custom-call | tf_op jit(solution)/shard_map/gather/pallas_call | solution.py:408
  61.6 5.9 %store.1 = (bf16[2048,2048]{1,0:T(8,128)(2,1)}, bf16[2048,2048]{1,0:T(8,128)(2,1)}) custom-call(bf16[2048,2048]{1,0:T(8,128)(2,1)S(1)} %get-tuple-element.8.up_ref, bf16[2048,2048]{1,0:T(8,128)(2,1)S(1)} %get-tuple-element.9.down_ref), custom_call_target="tpu_custom_call" | custom-call | tf_op jit(solution)/shard_map/store/pallas_call | solution.py:425
  67.6 47.7 %apply.1.refs_0_ = bf16[1536,512]{1,0:T(8,128)(2,1)S(1)} custom-call(bf16[2048,2048]{1,0:T(8,128)(2,1)S(1)} %get-tuple-element.8.up_ref, bf16[2048,2048]{1,0:T(8,128)(2,1)S(1)} %get-tuple-element.9.down_ref, bf16[4,1536,512]{2,1,0:T(8,128)(2,1)S(1)} %get-tuple-element.10.all_ref, bf16[2048,2048]{1,0:T(8,128)(2,1)} %get-tuple-element.11.stored_ref.refs_1_), custom_call_target="tpu_custom_call" | custom-call | tf_op jit(solution)/shard_map/apply/pallas_call | solution.py:435
  115.3 1.2 %finish.1 = (bf16[2048,2048]{1,0:T(8,128)(2,1)}, bf16[2048,2048]{1,0:T(8,128)(2,1)}, bf16[1536,512]{1,0:T(8,128)(2,1)}) custom-call(bf16[2048,2048]{1,0:T(8,128)(2,1)S(1)} %get-tuple-element.8.up_ref, bf16[2048,2048]{1,0:T(8,128)(2,1)S(1)} %get-tuple-element.9.down_ref, ...), custom_call_target="tpu_custom_call", output_to_operand_aliasing={{0}: (3, {}), {1}: (4, {})} | custom-call | tf_op jit(solution)/shard_map/finish/pallas_call | solution.py:447

commit v4 on v3

--- a/solution.py
+++ b/solution.py
@@ -9,12 +9,14 @@
 
 epsilon = 1e-06
 RING = 4
-HALF = 32
+UNIT = 16
 PIECE = 128
-LAG = 3
+LAG = 5
 TOKEN_LAG = 6
-TURN = 2
-PACE = {0: (2,) * 3 + (1,) * 12, 1: (0,) * 3 + (1,) * 12}
+TURN = 6
+PACE = ((1,) * 6 + (1, 0) * 13, (0,) * 7 + (1, 0) * 12 + (0,))
+READY = 18
+HIDE = ({18 + 2 * i: i for i in range(6)}, {22: 0, 26: 1, 30: 2})
 CHUNK = 256
 MESH = pl.DeviceIdType.MESH
 F32, BF16 = jnp.float32, jnp.bfloat16
@@ -42,14 +44,15 @@
     queues = {link: [] for link in links}
 
     def offer(unit, slot):
-        matrix, z, y, half = unit
-        first, second = ("y", "z") if matrix == 0 else ("z", "y")
+        matrix, order, z, y, half = unit
+        first, second = ("y", "z") if order == 0 else ("z", "y")
         for link in onward({"z": z, "y": y}, first, second, half):
-            queues[link].append((0 if link[0] == first else 1, slot, unit))
+            queues[link].append((matrix, 0 if link[0] == first else 1, slot, unit))
 
     for half in (0, 1):
         for matrix in (0, 1):
-            offer((matrix, 0, 0, half), 0)
+            for order in (0, 1):
+                offer((matrix, order, 0, 0, half), 0)
     slots, landed = [], {}
     while any(queues.values()) or any(landed.values()):
         now = len(slots)
@@ -58,23 +61,26 @@
         leaving = []
         for link in links:
             if queues[link]:
-                choice = min(queues[link], key=lambda entry: entry[:2])
+                choice = min(queues[link], key=lambda entry: entry[:3])
                 queues[link].remove(choice)
-                leaving.append((link, choice[2]))
-        landed[now] = []
-        for (axis, sign), (matrix, z, y, half) in leaving:
-            landed[now].append((matrix, z + sign * (axis == "z"), y + sign * (axis == "y"), half))
+                leaving.append((link, choice[3]))
+        landed[now] = [arrived(link, unit) for link, unit in leaving]
         slots.append(leaving)
-        if len(slots) > 100:
-            raise ValueError("plan")
     while slots and not slots[-1]:
         slots.pop()
     return slots
 
 
-def token_plan(pieces):
-    evens, odds = list(range(0, pieces, 2)), list(range(1, pieces, 2))
-    own = {1: evens + odds, -1: odds + evens}
+def arrived(link, unit):
+    (axis, sign), (matrix, order, z, y, half) = link, unit
+    return (matrix, order, z + sign * (axis == "z"), y + sign * (axis == "y"), half)
+
+
+def token_plan(pieces, sorted_first):
+    own = {sign: list(range(pieces)) for sign in (1, -1)}
+    if sorted_first:
+        for sign in own:
+            own[sign].sort(key=lambda piece: (piece % 2 == 0) != (sign == 1))
     passing = {1: [], -1: []}
     slots, landed = [], {}
     while own[1] or own[-1] or passing[1] or passing[-1] or any(landed.values()):
@@ -106,8 +112,8 @@
 
 
 def gather_kernel(
-    weights, token_slots, tok_ref, gain_in, up_in, down_in, up_ref, down_ref, all_ref,
-    gain_ref, up_own, down_own, w_recv, t_recv, w_send, t_send, p_send, p_recv, own_sem,
+    weights, token_slots, tok_ref, gain_in, up_in, down_in, up_ref, down_ref, hidden_ref,
+    all_ref, gain_ref, up_own, down_own, w_recv, t_recv, w_send, t_send, p_send, p_recv, own_sem,
 ):
     z, y, core, x = place()
     loads = [
@@ -134,10 +140,10 @@
     tables = (up_ref, down_ref)
 
     def weight_rows(unit):
-        matrix, hz, hy, half = unit
+        matrix, order, hz, hy, half = unit
         source = (turn(z, -hz) * RING + turn(y, -hy)) * 2 + core
-        start = pl.multiple_of(source * rows + half * HALF, HALF)
-        return tables[matrix].at[pl.ds(start, HALF), :]
+        start = pl.multiple_of(source * rows + (order * 2 + half) * UNIT, UNIT)
+        return tables[matrix].at[pl.ds(start, UNIT), :]
 
     def weight_copy(index, link, unit):
         ref = weight_rows(unit)
@@ -158,53 +164,48 @@
     for leaving in weights:
         for entry in leaving:
             w_index[entry] = len(w_index)
-    t_index = {}
-    for leaving in token_slots:
-        for entry in leaving:
-            t_index[entry] = len(t_index)
+    t_index = {entry: i for i, entry in enumerate(sorted(sum(token_slots[0], [])))}
 
     def send_weights(slot):
         if slot < len(weights):
             for link, unit in weights[slot]:
                 weight_copy(w_index[link, unit], link, unit).start()
 
-    def send_tokens(slot):
-        if slot < len(token_slots):
-            for entry in token_slots[slot]:
+    def send_tokens(which, slot):
+        if slot < len(token_slots[which]):
+            for entry in token_slots[which][slot]:
                 token_copy(t_index[entry], *entry).start()
 
     def receive_weights(slot):
         for link, unit in weights[slot]:
-            matrix, hz, hy, half = unit
-            got = (matrix, hz + link[1] * (link[0] == "z"), hy + link[1] * (link[0] == "y"), half)
+            got = arrived(link, unit)
             ref = weight_rows(got)
             pltpu.make_async_remote_copy(
                 ref, ref, w_send, w_recv.at[w_index[link, unit]], device(other=True), MESH
             ).wait_recv()
             partner_copy(got).start()
 
-    def receive_tokens(slot):
-        for sign, hops, piece in token_slots[slot]:
+    def receive_tokens(which, slot):
+        for sign, hops, piece in token_slots[which][slot]:
             at = pl.ds(piece * PIECE, PIECE)
             ref = all_ref.at[turn(x, -sign * (hops + 1)), at, :]
             pltpu.make_async_remote_copy(
                 ref, ref, t_send, t_recv.at[t_index[sign, hops, piece]], device(other=True), MESH
             ).wait_recv()
 
-    def first_tokens():
+    def first_tokens(which):
         for slot in range(TOKEN_LAG):
-            send_tokens(slot)
-
-    def next_tokens(slot):
-        if slot < len(token_slots):
-            receive_tokens(slot)
-            send_tokens(slot + TOKEN_LAG)
+            send_tokens(which, slot)
+
+    def next_tokens(which, slot):
+        receive_tokens(which, slot)
+        send_tokens(which, slot + TOKEN_LAG)
 
     pl.semaphore_wait(barrier, len(neighbours))
 
     @pl.when(core == 0)
     def _():
-        first_tokens()
+        first_tokens(0)
 
     mine = pl.ds(pl.multiple_of(((z * RING + y) * 2 + core) * rows, rows), rows)
     square = (rows, rows)
@@ -217,49 +218,70 @@
     for slot in range(LAG):
         send_weights(slot)
     for matrix in (0, 1):
-        for half in (0, 1):
-            partner_copy((matrix, 0, 0, half)).start()
-    done = {0: 0, 1: 0}
+        for order in (0, 1):
+            for half in (0, 1):
+                partner_copy((matrix, order, 0, 0, half)).start()
+
+    def settle(ref, sem):
+        pltpu.make_async_copy(ref, ref, sem).wait()
+
+    half_rows = up_ref.shape[0] // 2
+    done = [0, 0]
+
+    def advance(which, count):
+        count = min(count, len(token_slots[which]) - done[which])
+        for slot in range(done[which], done[which] + count):
+            next_tokens(which, slot)
+        done[which] += count
+
     for slot in range(len(weights)):
         receive_weights(slot)
         send_weights(slot + LAG)
         for which in (0, 1):
-            steps = range(done[which], min(done[which] + PACE[which][slot], len(token_slots)))
-            done[which] = max(done[which], steps.stop)
-            if steps or (which == 1 and slot == TURN):
-
-                @pl.when(core == which)
-                def _(slot=slot, which=which, steps=steps):
-                    if which == 1 and slot == TURN:
-                        first_tokens()
-                    for step in steps:
-                        next_tokens(step)
-
-    for which in (0, 1):
-
-        @pl.when(core == which)
-        def _(which=which):
-            for step in range(done[which], len(token_slots)):
-                next_tokens(step)
-
-    def settle(ref, sem):
-        pltpu.make_async_copy(ref, ref, sem).wait()
-
-    loads[3].wait()
-    half_rows = up_ref.shape[0] // 2
-    for matrix in (0, 1):
-        settle(tables[matrix].at[pl.ds(0, half_rows), :], p_recv.at[matrix])
+
+            @pl.when(core == which)
+            def _(slot=slot, which=which):
+                if which == 1 and slot == TURN:
+                    first_tokens(which)
+                advance(which, PACE[which][slot])
+
+        if slot == READY:
+            loads[3].wait()
+            settle(up_ref.at[pl.ds(0, half_rows), :], p_recv.at[0])
+        if slot in HIDE[0] and slot in HIDE[1]:
+            hide(all_ref, up_ref, hidden_ref, jnp.where(core == 0, HIDE[0][slot], HIDE[1][slot]))
+        elif slot in HIDE[0] or slot in HIDE[1]:
+            which = 0 if slot in HIDE[0] else 1
+
+            @pl.when(core == which)
+            def _(step=HIDE[which][slot]):
+                hide(all_ref, up_ref, hidden_ref, step)
+
+    @pl.when(core == 0)
+    def _():
+        advance(0, len(token_slots[0]))
+
+    @pl.when(core == 1)
+    def _():
+        for step in range(len(HIDE[1]), hidden_ref.shape[0] // CHUNK):
+            last = max(i for i, leaving in enumerate(token_slots[1]) for entry in leaving if entry[2] * PIECE // CHUNK == step)
+            advance(1, last + 1 - done[1])
+            hide(all_ref, up_ref, hidden_ref, step)
+        advance(1, len(token_slots[1]))
+
+    settle(down_ref.at[pl.ds(0, half_rows), :], p_recv.at[1])
     for matrix in (0, 1):
         settle(tables[matrix].at[pl.ds(0, half_rows), :], p_send)
-        settle(tables[matrix].at[pl.ds(0, len(w_index) // 2 * HALF), :], w_send)
+        settle(tables[matrix].at[pl.ds(0, len(w_index) // 2 * UNIT), :], w_send)
     for _ in range(len(t_index) * PIECE // all_ref.shape[1]):
         settle(all_ref.at[0], t_send)
 
 
-def products(x, all_ref, up_ref, down_ref, hidden_ref, at):
+def hide(all_ref, up_ref, hidden_ref, step):
     sources, _, width = all_ref.shape
     features, units = up_ref.shape
     tile = 512
+    at = pl.ds(step * CHUNK if isinstance(step, int) else pl.multiple_of(step * CHUNK, CHUNK), CHUNK)
     pieces = [all_ref[k, at, :].astype(F32) for k in range(sources)]
     total = sum(jnp.sum(p * p, axis=-1, keepdims=True) for p in pieces)
     scale = lax.rsqrt(total * (1.0 / features) + epsilon)
@@ -269,15 +291,7 @@
         acc = jnp.zeros((CHUNK, tile), F32)
         for k in range(sources):
             acc += jnp.dot(normed[k], up_ref[pl.ds(k * width, width), cols], preferred_element_type=F32)
-        hidden_ref[:, cols] = jnp.square(jnp.maximum(acc, 0.0)).astype(BF16)
-
-    def block(by):
-        cols = pl.ds(pl.multiple_of(turn(x, by) * width, width), width)
-        return lax.dot_general(
-            hidden_ref[...], down_ref[cols, :], (((1,), (1,)), ((), ())), preferred_element_type=F32
-        ).astype(BF16)
-
-    return block
+        hidden_ref[at, cols] = jnp.square(jnp.maximum(acc, 0.0)).astype(BF16)
 
 
 TARGETS = (2, 1, -1, 0)
@@ -309,8 +323,8 @@
 
 
 def apply_kernel(
-    up_ref, down_ref, all_ref, stored_ref, out_ref,
-    hidden_ref, far_ref, right_ref, left_ref, mine_ref, far_left, far_right, from_left, from_right,
+    up_ref, down_ref, hidden_ref, stored_ref, out_ref,
+    far_ref, right_ref, left_ref, mine_ref, far_left, far_right, from_left, from_right,
     send_sem, far_recv, near_recv,
 ):
     z, y, core, x = place()
@@ -362,7 +376,13 @@
 
     def multiply(step, first):
         at = span(step)
-        block = products(x, all_ref, up_ref, down_ref, hidden_ref, at)
+
+        def block(by):
+            cols = pl.ds(pl.multiple_of(turn(x, by) * width, width), width)
+            return lax.dot_general(
+                hidden_ref[at, :], down_ref[cols, :], (((1,), (1,)), ((), ())), preferred_element_type=F32
+            ).astype(BF16)
+
         far_ref[at, :] = block(TARGETS[0])
         if first:
             pl.semaphore_wait(barrier, 2)
@@ -399,21 +419,21 @@
 def on_device(tokens, norm_gain, up_weight, down_weight):
     count, width = tokens.shape
     features, units = width * RING, up_weight.shape[1]
-    weights, token_slots = weight_plan(), token_plan(count // PIECE)
+    weights, token_slots = weight_plan(), [token_plan(count // PIECE, which == 0) for which in (0, 1)]
     steps = count // CHUNK
     vmem, hbm = pl.BlockSpec(memory_space=pltpu.VMEM), pl.BlockSpec(memory_space=pltpu.HBM)
     dma = pltpu.SemaphoreType.DMA
     matrix = (features, units)
-    hidden = pltpu.VMEM((CHUNK, units), BF16)
-    up, down, gathered = pl.pallas_call(
+    up, down, hidden = pl.pallas_call(
         functools.partial(gather_kernel, weights, token_slots),
         name="gather",
-        out_shape=[pltpu.VMEM(matrix, BF16), pltpu.VMEM(matrix, BF16), pltpu.VMEM((RING, count, width), BF16)],
+        out_shape=[pltpu.VMEM(matrix, BF16), pltpu.VMEM(matrix, BF16), pltpu.VMEM((count, units), BF16)],
         in_specs=[hbm] * 4,
         out_specs=[vmem] * 3,
         scratch_shapes=[
+            pltpu.VMEM((RING, count, width), BF16),
             pltpu.VMEM((1, norm_gain.shape[0]), F32), pltpu.VMEM(up_weight.shape, F32), pltpu.VMEM(up_weight.shape, F32),
-            dma((sum(map(len, weights)),)), dma((sum(map(len, token_slots)),)), dma, dma, dma, dma((2,)), dma((4,)),
+            dma((sum(map(len, weights)),)), dma((sum(map(len, token_slots[0])),)), dma, dma, dma, dma((2,)), dma((4,)),
         ],
         compiler_params=pltpu.CompilerParams(collective_id=0, has_side_effects=True, vmem_limit_bytes=33 * 2**20),
     )(tokens, norm_gain[None, :], up_weight, down_weight)
@@ -439,11 +459,11 @@
         in_specs=[vmem] * 3 + [hbm],
         out_specs=vmem,
         scratch_shapes=[
-            hidden, rows, rows, rows, rows, half_rows, half_rows, rows, rows,
+            rows, rows, rows, rows, half_rows, half_rows, rows, rows,
             dma, dma((steps, 2)), dma((steps, 2, 2)),
         ],
         compiler_params=pltpu.CompilerParams(collective_id=1, has_side_effects=True, vmem_limit_bytes=31 * 2**20),
-    )(*pinned(up, down, gathered), stored[0])
+    )(*pinned(up, down, hidden), stored[0])
     return pl.pallas_call(
         functools.partial(store_kernel, 0),
         name="finish",

time: 117 us -> 116 us (level)
    pallas_call x1, Pallas kernels: 47.7 us -> 42.4 us  [on_device(): pl.pallas_call(apply_kernel, name='apply', out_shape=pltpu.VMEM((count, w...]
    pallas_call x1, Pallas kernels: 61 us -> 65.5 us  [on_device(): pl.pallas_call(functools.partial(gather_kernel, weights, token_slots), na...]
where the time goes in v4:
time: 116 us
  Pallas kernels  115 us (99%)
    pallas_call x1, Pallas kernels, on_device(): pl.pallas_call(functools.partial(gather_kernel, weights, token_slots), na...  65.5 us
    pallas_call x1, Pallas kernels, on_device(): pl.pallas_call(apply_kernel, name='apply', out_shape=pltpu.VMEM((count, w...  42.4 us
    pallas_call x1, Pallas kernels, on_device(): pl.pallas_call(functools.partial(store_kernel, 1), name='store', out_shap...  5.94 us

profile of v4, /device:TPU:1, one launch (start us, length us, event | category | flops | bytes accessed | tf_op | source)
XLA Modules:
  0.0 115.9 jit_solution(221866496671143752)
XLA Ops:
  0.6 65.5 %gather.1 = (bf16[2048,2048]{1,0:T(8,128)(2,1)S(1)}, bf16[2048,2048]{1,0:T(8,128)(2,1)S(1)}, bf16[1536,2048]{1,0:T(8,128)(2,1)S(1)}) custom-call(bf16[1536,512]{1,0:T(8,128)(2,1)} %tok_ref.1, f32[1,64]{1,0:T(1,128)} %bitcast.1, f32[64,2048]{1,0:T(8,128)} %up_in.1, f32[64,2048]{1,0:T(8,128)} %down_in.1), custom_call_target="tpu_custom_call" | custom-call | tf_op jit(solution)/shard_map/gather/pallas_call | solution.py:427
  66.2 5.9 %store.1 = (bf16[2048,2048]{1,0:T(8,128)(2,1)}, bf16[2048,2048]{1,0:T(8,128)(2,1)}) custom-call(bf16[2048,2048]{1,0:T(8,128)(2,1)S(1)} %get-tuple-element.8.up_ref, bf16[2048,2048]{1,0:T(8,128)(2,1)S(1)} %get-tuple-element.9.down_ref), custom_call_target="tpu_custom_call" | custom-call | tf_op jit(solution)/shard_map/store/pallas_call | solution.py:445
  72.1 42.4 %apply.1.refs_0_ = bf16[1536,512]{1,0:T(8,128)(2,1)S(1)} custom-call(bf16[2048,2048]{1,0:T(8,128)(2,1)S(1)} %get-tuple-element.8.up_ref, bf16[2048,2048]{1,0:T(8,128)(2,1)S(1)} %get-tuple-element.9.down_ref, bf16[1536,2048]{1,0:T(8,128)(2,1)S(1)} %get-tuple-element.10.hidden_ref, bf16[2048,2048]{1,0:T(8,128)(2,1)} %get-tuple-element.11.stored_ref.refs_1_), custom_call_target="tpu_custom_call" | custom-call | tf_op jit(solution)/shard_map/apply/pallas_call | solution.py:455
  114.5 1.2 %finish.1 = (bf16[2048,2048]{1,0:T(8,128)(2,1)}, bf16[2048,2048]{1,0:T(8,128)(2,1)}, bf16[1536,512]{1,0:T(8,128)(2,1)}) custom-call(bf16[2048,2048]{1,0:T(8,128)(2,1)S(1)} %get-tuple-element.8.up_ref, bf16[2048,2048]{1,0:T(8,128)(2,1)S(1)} %get-tuple-element.9.down_ref, ...), custom_call_target="tpu_custom_call", output_to_operand_aliasing={{0}: (3, {}), {1}: (4, {})} | custom-call | tf_op jit(solution)/shard_map/finish/pallas_call | solution.py:467
